TPU v7x, 32 devices: a whole 2x2x4 slice. The times are simulated.
32 devices in a mesh: ep: 8 (over z, y), tp: 4 (over x, core).
Axes of the slice: x: 2, y: 2, z: 4, core: 2. Of those that a mesh axis runs over, the one named last changes fastest.
Arguments:
- q_heads: bfloat16 [8192, 1024], P('ep', 'tp'), may hold values from -200 to 200
- k_heads: bfloat16 [8192, 256], P('ep', 'tp'), may hold values from -6 to 6
- v_heads: bfloat16 [8192, 256], P('ep', 'tp'), may hold values from -6 to 6
- sink_logits: float32 [16], P('tp'), may hold values from 1 to 5
- out_weight: bfloat16 [1024, 2048], P(None, 'tp'), may hold values from -1.5 to 1.5
- tokens_b: bfloat16 [4096, 2048], P('ep'), may hold values from -6 to 6
- moe_gain: float32 [2048], replicated, may hold values from 0.1 to 1.9
- router_group: bfloat16 [2048, 4], replicated, may hold values from -0.125 to 0.125
- router_expert: bfloat16 [2048, 16], replicated, may hold values from -0.125 to 0.125
- route_expert: int32 [4096, 2], P('ep'), may hold values from 0 to 15, as said below
- expert_gate: bfloat16 [16, 2048, 1024], P('ep', None, 'tp'), may hold values from -0.125 to 0.125
- expert_up: bfloat16 [16, 2048, 1024], P('ep', None, 'tp'), may hold values from -0.125 to 0.125
- expert_down: bfloat16 [16, 1024, 2048], P('ep', 'tp'), may hold values from -0.75 to 0.75
Outputs:
- mixer_out: bfloat16 [8192, 2048], P('ep', 'tp')
- moe_out: bfloat16 [4096, 2048], P(('ep', 'tp'))
Inputs may be any that keep to these rules, and one draw needn't show every extreme that they name: `route_expert`: each token names two different experts, in rising order, of one group of 4 consecutive experts. In each aligned block of 128 rows (the rows of one device) no expert is named by more than 32 tokens, in each group one expert is named by exactly 32 tokens of every block, and each group is named by a quarter of every block's tokens.
All inputs are finite; a program needn't handle non-finite values.
Results may differ from a plain program's by a relative error of at most 0.011.
Values may be sent and summed in bfloat16 or wider, within the bound.
No kernel may reach another device: no remote copies, remote signals or barrier semaphores. Data moves between devices by JAX's collectives and lax.ppermute only.
A program may use at most 128 MiB of HBM per device.

v0:
```python
import jax
import jax.numpy as jnp
from jax import lax
from jax.sharding import PartitionSpec as P

HEADS = 16
KV = 4
HD = 64
WINDOW = 128


def shifted(value, axis, steps):
    count = lax.axis_size(axis)
    leading, last = (max(0, -steps), min(count, count - steps))
    return lax.ppermute(value, axis, [(source, source + steps) for source in range(leading, last)])


def normalize(rows_in, gain):
    values = rows_in.astype(jnp.float32)
    scaled = values * lax.rsqrt(jnp.mean(values * values, axis=-1, keepdims=True) + 1e-06) * gain
    return scaled.astype(jnp.bfloat16)


def gate_weights(normed, routes, router_group, router_expert):
    group_logits = jnp.dot(normed, router_group, preferred_element_type=jnp.float32)
    expert_logits = jnp.dot(normed, router_expert, preferred_element_type=jnp.float32)
    group_count = router_group.shape[1]
    expert_count = router_expert.shape[1]
    chosen_group = routes[:, 0] // (expert_count // group_count)
    group_match = chosen_group[:, None] == jnp.arange(group_count, dtype=jnp.int32)[None, :]
    group_share = jnp.sum(
        jnp.where(group_match, jax.nn.softmax(group_logits, axis=-1), 0.0), axis=-1
    )
    expert_match = routes[:, :, None] == jnp.arange(expert_count, dtype=jnp.int32)[None, None, :]
    picked = jnp.sum(jnp.where(expert_match, expert_logits[:, None, :], 0.0), axis=-1)
    return group_share[:, None] * jax.nn.softmax(picked, axis=-1)


def slot_positions(routes, sub_count, expert_count):
    flat_routes = routes.reshape(sub_count, -1)
    onehot = (
        flat_routes[:, :, None] == jnp.arange(expert_count, dtype=jnp.int32)[None, None, :]
    ).astype(jnp.int32)
    places = jnp.sum(onehot * jnp.cumsum(onehot, axis=1), axis=2) - 1
    return (flat_routes, places)


def fill_slots(normed, flat_routes, places, sub_count, expert_count, capacity, exp_local):
    sub_index = jnp.arange(sub_count, dtype=jnp.int32)[:, None]
    target = ((flat_routes * sub_count + sub_index) * capacity + places).reshape(-1)
    source = jnp.repeat(normed, 2, axis=0)
    buffer = jnp.zeros((expert_count * sub_count * capacity, normed.shape[1]), jnp.bfloat16)
    buffer = buffer.at[target].set(source)
    return buffer.reshape(
        expert_count // exp_local, exp_local, sub_count, capacity, normed.shape[1]
    )


def per_device(
    q_heads,
    k_heads,
    v_heads,
    sink_logits,
    out_weight,
    tokens_b,
    moe_gain,
    router_group,
    router_expert,
    route_expert,
    expert_gate,
    expert_up,
    expert_down,
):
    span_len = WINDOW
    row_count = q_heads.shape[0]
    kv_local = k_heads.shape[1] // HD
    group_size = HEADS // KV
    blocks = row_count // span_len
    stacked = jnp.stack([k_heads[row_count - span_len :], v_heads[row_count - span_len :]])
    earlier = shifted(stacked, "ep", 1)

    def make_band(own_rows, prev_rows):
        extended = jnp.concatenate([prev_rows, own_rows], axis=0).reshape(
            blocks + 1, span_len, kv_local, HD
        )
        return jnp.concatenate([extended[:-1], extended[1:]], axis=1)

    key_band = make_band(k_heads, earlier[0])
    value_band = make_band(v_heads, earlier[1])
    query_blocks = q_heads.reshape(blocks, span_len, kv_local, group_size, HD)
    scores = jnp.einsum(
        "nqhgd,nkhd->nhgqk", query_blocks, key_band, preferred_element_type=jnp.float32
    ) * HD ** (-0.5)
    first_row = lax.axis_index("ep") * row_count
    query_index = jnp.arange(span_len, dtype=jnp.int32)[:, None]
    key_index = jnp.arange(2 * span_len, dtype=jnp.int32)[None, :]
    distance = query_index + span_len - key_index
    key_place = (
        first_row
        + jnp.arange(blocks, dtype=jnp.int32)[:, None, None] * span_len
        + key_index[None]
        - span_len
    )
    allowed = (distance >= 0)[None] & (distance < span_len)[None] & (key_place >= 0)
    masked = jnp.where(allowed[:, None, None], scores, -1e30)
    sink_full = sink_logits.reshape(kv_local, group_size)[None, :, :, None]
    row_max = jnp.maximum(jnp.max(masked, axis=-1), sink_full)
    weights_exp = jnp.exp(masked - row_max[..., None])
    denominator = jnp.sum(weights_exp, axis=-1) + jnp.exp(sink_full - row_max)
    probs = (weights_exp / denominator[..., None]).astype(jnp.bfloat16)
    attended = jnp.einsum(
        "nhgqk,nkhd->nqhgd", probs, value_band, preferred_element_type=jnp.float32
    )
    attended = attended.astype(jnp.bfloat16).reshape(row_count, kv_local * group_size * HD)
    mixed = jnp.dot(
        lax.all_gather(attended, "tp", axis=1, tiled=True),
        out_weight,
        preferred_element_type=jnp.float32,
    )
    mixer_out = mixed.astype(jnp.bfloat16)
    tp_count = lax.axis_size("tp")
    tp_index = lax.axis_index("tp")
    exp_local = expert_gate.shape[0]
    expert_count = exp_local * lax.axis_size("ep")
    rows_dev = tokens_b.shape[0] // tp_count
    capacity = min(4 * rows_dev // expert_count, rows_dev // 4)
    own_routes = lax.dynamic_slice_in_dim(route_expert, tp_index * rows_dev, rows_dev, 0)
    own_normed = normalize(
        lax.dynamic_slice_in_dim(tokens_b, tp_index * rows_dev, rows_dev, 0), moe_gain
    )
    flat_routes, places = slot_positions(own_routes, 1, expert_count)
    buffer = fill_slots(own_normed, flat_routes, places, 1, expert_count, capacity, exp_local)
    delivered = lax.all_to_all(buffer, "ep", split_axis=0, concat_axis=0, tiled=True)
    arrived = lax.all_gather(delivered, "tp", axis=2, tiled=True)
    own_flat = flat_routes[0]
    own_places = places[0]
    gates = gate_weights(own_normed, own_routes, router_group, router_expert)
    gate_pre = jnp.einsum(
        "setcd,edf->setcf", arrived, expert_gate, preferred_element_type=jnp.float32
    )
    up_pre = jnp.einsum("setcd,edf->setcf", arrived, expert_up, preferred_element_type=jnp.float32)
    activated = (jax.nn.silu(gate_pre) * up_pre).astype(jnp.bfloat16)
    partial_value = jnp.einsum(
        "setcf,efd->setcd", activated, expert_down, preferred_element_type=jnp.float32
    )
    summed = lax.psum_scatter(
        partial_value.astype(jnp.bfloat16), "tp", scatter_dimension=2, tiled=True
    )
    returned = lax.all_to_all(summed, "ep", split_axis=0, concat_axis=0, tiled=True)
    returned = returned.reshape(expert_count * capacity, returned.shape[-1])
    picked_rows = returned[own_flat * capacity + own_places].reshape(
        rows_dev, 2, returned.shape[-1]
    )
    moe_out = jnp.sum(gates[:, :, None] * picked_rows.astype(jnp.float32), axis=1).astype(
        jnp.bfloat16
    )
    return (mixer_out, moe_out)


def solution(mesh):
    in_specs = (
        P("ep", "tp"),
        P("ep", "tp"),
        P("ep", "tp"),
        P("tp"),
        P(None, "tp"),
        P("ep", None),
        P(),
        P(),
        P(),
        P("ep", None),
        P("ep", None, "tp"),
        P("ep", None, "tp"),
        P("ep", "tp", None),
    )
    out_specs = (P("ep", "tp"), P(("ep", "tp"), None))
    return jax.shard_map(
        per_device, mesh=mesh, in_specs=in_specs, out_specs=out_specs, check_vma=False
    )
```

profile of v0, /device:TPU:0, one launch (start us, length us, event | category | flops | bytes accessed | tf_op | source)
XLA Modules:
  0.0 384.7 jit_solution(17518008943013169215)
XLA Ops:
  7.2 0.8 broadcast_multiply_fusion
  8.3 0.6 reduce-window.6
  9.7 1.2 fusion.24
  10.9 1.3 fusion.26
  12.2 1.6 broadcast_in_dim.34
  13.8 2.3 reshape.383
  16.0 4.4 %scatter_custom_fusion = bf16[512,2048]{1,0:T(8,128)(2,1)} fusion(s32[256]{0:T(256)S(1)} %bitcast.171, bf16[256,2048]{1,0:T(8,128)(2,1)} %reshape.383, bf16[]{:T(256)} %constant.67.clone.1), kind=kCustom, calls=%fused_computation.35 | custom fusion | bytes 2097664 | tf_op jit(solution)/shard_map/scatter | solution.py:53
  20.5 55.5 %all_to_all.10 = bf16[8,2,1,32,2048]{4,3,2,1,0:T(8,128)(2,1)S(1)} all-to-all(bf16[8,2,1,32,2048]{4,3,2,1,0:T(8,128)(2,1)} %bitcast.159), channel_id=1, replica_groups=mesh['ep'=8,'tp'=4] {'ep'}, dimensions={0} | all-to-all | bytes 4194304 | tf_op jit(solution)/shard_map/all_to_all | solution.py:133
  76.0 1.5 copy.69
  77.6 57.4 %all-gather.5.cloned.1.call-done = bf16[8,2,4,32,2048]{4,3,2,0,1:T(8,128)(2,1)} async-done(((bf16[8,2,1,32,2048]{4,3,2,0,1:T(8,128)(2,1)}), bf16[8,2,4,32,2048]{4,3,2,0,1:T(8,128)(2,1)}) %all-gather.5.cloned.1.call-update) | async-done | bytes 8388624 | tf_op jit(solution)/shard_map/all_gather | solution.py:134
  134.9 7.7 %fusion.3 = f32[2,8,4,32,256]{4,3,2,1,0:T(8,128)} fusion(bf16[8,2,4,32,2048]{4,3,2,0,1:T(8,128)(2,1)} %all-gather.5.cloned.1.call-done, bf16[2,2048,256]{2,1,0:T(8,128)(2,1)} %param.24), kind=kOutput, calls=%fused_computation.9 | convolution fusion | flops 2147483648 | bytes 12582912 | tf_op jit(solution)/shard_map/setcd,edf->setcf/dot_general | solution.py:141
  142.6 13.5 %convert_bitcast_fusion = bf16[8,2,4,32,2048]{4,3,2,0,1:T(8,128)(2,1)} fusion(bf16[2,256,2048]{2,1,0:T(8,128)(2,1)S(1)} %copy-done, f32[2,8,4,32,256]{4,3,2,1,0:T(8,128)} %fusion.3, bf16[8,2,4,32,2048]{4,3,2,0,1:T(8,128)(2,1)} %all-gather.5.cloned.1.call-done, bf16[2,2048,256]{2,1,0:T(8,128)(2,1)} %param.23), kind=kOutput, calls=%fused_computation.2 | convolution fusion | flops 4302307328 | bytes 23068672 | tf_op jit(solution)/shard_map/setcf,efd->setcd/dot_general | solution.py:143
  156.1 0.9 copy-done.3
  157.1 3.6 collective-permute-start
  161.2 0.4 reshape.392
  161.7 0.6 dynamic-slice
  162.5 0.9 fusion.1
  163.5 1.1 fusion
  164.5 0.8 copy-done.2
  165.4 143.8 %all-reduce.3.cloned.1.call-done = bf16[8,2,4,32,2048]{4,3,2,0,1:T(8,128)(2,1)} async-done(((bf16[8,2,4,32,2048]{4,3,2,0,1:T(8,128)(2,1)}), bf16[8,2,4,32,2048]{4,3,2,0,1:T(8,128)(2,1)}) %all-reduce.3.cloned.1.call-update) | async-done | bytes 8388624
  309.2 2.5 constant_dynamic-slice_fusion
  311.6 1.6 copy.70
  313.2 5.5 %all-to-all-start.1 = ((bf16[8,2,1,32,2048]{4,3,2,1,0:T(8,128)(2,1)}), bf16[8,2,1,32,2048]{4,3,2,1,0:T(8,128)(2,1)S(1)}, u32[]{:S(2)}, u32[]{:S(2)}) async-start(bf16[8,2,1,32,2048]{4,3,2,1,0:T(8,128)(2,1)} %copy.70), calls=%async_computation.1 | async-start | bytes 4194304 | tf_op jit(solution)/shard_map/all_to_all | solution.py:149
  318.8 3.4 fusion.21
  322.2 0.3 copy.61
  322.6 0.9 copy.91
  324.3 22.5 %all-gather.3.cloned.1.call-done = bf16[1024,1024]{0,1:T(8,128)(2,1)} async-done(((bf16[1024,256]{0,1:T(8,128)(2,1)}), bf16[1024,1024]{0,1:T(8,128)(2,1)}) %all-gather.3.cloned.1.call-update) | async-done | bytes 2097168 | tf_op jit(solution)/shard_map/all_gather | solution.py:116
  346.8 4.1 %convolution_convert_fusion = bf16[1024,512]{1,0:T(8,128)(2,1)} fusion(bf16[1024,1024]{0,1:T(8,128)(2,1)} %all-gather.3.cloned.1.call-done, bf16[1024,512]{1,0:T(8,128)(2,1)} %param.17), kind=kOutput, calls=%fused_computation.24 | convolution fusion | flops 1074266112 | bytes 4194304 | tf_op jit(solution)/shard_map/dot_general | solution.py:115
  350.9 15.8 %all-to-all-done.1 = bf16[8,2,1,32,2048]{4,3,2,1,0:T(8,128)(2,1)S(1)} async-done(((bf16[8,2,1,32,2048]{4,3,2,1,0:T(8,128)(2,1)}), bf16[8,2,1,32,2048]{4,3,2,1,0:T(8,128)(2,1)S(1)}, u32[]{:S(2)}, u32[]{:S(2)}) %all-to-all-start.1) | async-done | bytes 2097184 | tf_op jit(solution)/shard_map/all_to_all | solution.py:149
  366.7 2.3 gather_fusion
  369.0 3.5 reshape.370
  372.6 5.6 %multiply_reduce_fusion = bf16[128,2048]{1,0:T(8,128)(2,1)} fusion(f32[128,2,2048]{2,1,0:T(2,128)} %reshape.370, f32[128,2]{1,0:T(8,128)S(1)} %copy.62), kind=kLoop, calls=%fused_computation.22 | loop fusion | flops 786432 | bytes 2622464 | tf_op jit(solution)/shard_map/reduce_sum | solution.py:154
  (72 shorter events, 2.9 us)
Async XLA Ops:
  7.2 135.4 %copy-start = (bf16[2,256,2048]{2,1,0:T(8,128)(2,1)S(1)}, bf16[2,256,2048]{2,1,0:T(8,128)(2,1)}, u32[]{:S(2)}) copy-start(bf16[2,256,2048]{2,1,0:T(8,128)(2,1)} %param.25) | copy-start | bytes 6291460
  7.2 127.8 %all-gather.5.cloned.1.call-start = ((), (), s32[]{:S(2)}) async-start(), calls=%async_computation.3 | async-start | bytes 10485760 | tf_op jit(solution)/shard_map/all_gather | solution.py:134
  77.5 231.6 %all-reduce.3.cloned.1.call-start = ((), (), s32[]{:S(2)}) async-start(), calls=%async_computation.4 | async-start | bytes 16777216
  156.1 0.9 copy-start.3
  156.1 1.0 copy-start.4
  156.1 5.1 %copy-start.5 = (bf16[1024,256]{1,0:T(8,128)(2,1)S(1)}, bf16[1024,256]{1,0:T(8,128)(2,1)}, u32[]{:S(2)}) copy-start(bf16[1024,256]{1,0:T(8,128)(2,1)} %param.13) | copy-start | bytes 1572868
  157.1 4.6 %copy-start.9 = (u32[32]{0:T(128)S(1)}, u32[32]{0:T(128)}, u32[]{:S(2)}) copy-start(u32[32]{0:T(128)} %constant.75) | copy-start | bytes 388
  157.1 5.2 %collective-permute-start = (bf16[2,128,64]{1,2,0:T(8,128)(2,1)S(1)}, bf16[2,128,64]{1,2,0:T(8,128)(2,1)S(1)}, u32[]{:S(2)}, u32[]{:S(2)}) collective-permute-start(bf16[2,128,64]{1,2,0:T(8,128)(2,1)S(1)} %pad_maximum_fusion.2), channel_id=1, source_target_pairs={{0,4},{4,8},{8,12},{12,16},{16,20},{20,24},{24,28},{1,5},{5,9},{9,... | collective-permute-start | bytes 98312 | tf_op jit(solution)/shard_map/ppermute | solution.py:15
  162.5 0.9 copy-start.8
  163.4 1.9 copy-start.2
  313.2 53.4 %all-to-all-start.1 = ((bf16[8,2,1,32,2048]{4,3,2,1,0:T(8,128)(2,1)}), bf16[8,2,1,32,2048]{4,3,2,1,0:T(8,128)(2,1)S(1)}, u32[]{:S(2)}, u32[]{:S(2)}) async-start(bf16[8,2,1,32,2048]{4,3,2,1,0:T(8,128)(2,1)} %copy.70), calls=%async_computation.1 | async-start | bytes 4194304 | tf_op jit(solution)/shard_map/all_to_all | solution.py:149
  318.8 28.0 %all-gather.3.cloned.1.call-start = ((), (), s32[]{:S(2)}) async-start(), calls=%async_computation.2 | async-start | bytes 2621440 | tf_op jit(solution)/shard_map/all_gather | solution.py:116
  322.2 1.3 copy-start.6
  322.2 1.6 copy-start.7
  369.0 9.1 %copy-start.1 = (bf16[2,256,2048]{2,1,0:T(8,128)(2,1)S(1)}, bf16[2,256,2048]{2,1,0:T(8,128)(2,1)}, u32[]{:S(2)}) copy-start(bf16[2,256,2048]{2,1,0:T(8,128)(2,1)} %param.25) | copy-start | bytes 6291460
Sparse Core Ops, SparseCore 0:
  77.6 57.2 all-gather.4
  156.3 152.8 all-reduce.2
  323.6 23.1 all-gather.2
where the time goes:
time: 385 us
  waiting for transfers between devices  239 us (62%)
  blocking collectives  55.5 us (14%)
  matrix products  30.1 us (8%)
  local copies, waits for them, and re-layouts  24.9 us (6%)
  between operations  14.1 us (4%)
  other arithmetic  11.5 us (3%)
  starting transfers between devices  9.2 us (2%)
    unnamed x4, waiting for transfers between devices  144 us
    all_gather x1, waiting for transfers between devices, per_device(): arrived = lax.all_gather(delivered, 'tp', axis=2, tiled=True)  57.4 us
    all_to_all x1, blocking collectives, per_device(): lax.all_to_all(buffer, 'ep', split_axis=0, concat_axis=0, tiled=True)  55.5 us
    all_gather x1, waiting for transfers between devices, per_device(): lax.all_gather(attended, 'tp', axis=1, tiled=True)  22.5 us
    all_to_all x1, waiting for transfers between devices, per_device(): lax.all_to_all(summed, 'ep', split_axis=0, concat_axis=0, tiled=True)  15.8 us
    dot_general x1, matrix products, per_device(): jnp.einsum('setcf,efd->setcd', activated, expert_down, preferred_element_...  13.5 us
  transfers between devices with their start and end apart: 5, of which 4 were waited for; matrix products, arithmetic and copies ran while one was open for 3% of the time, Pallas kernels for 0%

commit v1 on v0

--- a/solution.py
+++ b/solution.py
@@ -131,7 +131,12 @@
     flat_routes, places = slot_positions(own_routes, 1, expert_count)
     buffer = fill_slots(own_normed, flat_routes, places, 1, expert_count, capacity, exp_local)
     delivered = lax.all_to_all(buffer, "ep", split_axis=0, concat_axis=0, tiled=True)
-    arrived = lax.all_gather(delivered, "tp", axis=2, tiled=True)
+    ring = [delivered]
+    for hop in range(3):
+        ring.append(lax.ppermute(ring[-1], "tp", [(dev, (dev + 1) % 4) for dev in range(4)]))
+    arrived = jnp.roll(
+        jnp.concatenate(ring[::-1], axis=2), (lax.axis_index("tp") + 1) * ring[0].shape[2], axis=2
+    )
     own_flat = flat_routes[0]
     own_places = places[0]
     gates = gate_weights(own_normed, own_routes, router_group, router_expert)

time: 385 us -> 417 us (1.083)
  waiting for transfers between devices: 239 us -> 258 us
  local copies, waits for them, and re-layouts: 24.9 us -> 42.1 us
    ppermute x0 -> x3, waiting for transfers between devices: none -> 76.8 us  [per_device(): lax.ppermute(ring[-1], 'tp', [(dev, (dev + 1) % 4) for dev in range(4)])]
    all_gather x1 -> x0, waiting for transfers between devices: 57.4 us -> none  [per_device(): arrived = lax.all_gather(delivered, 'tp', axis=2, tiled=True)]
    unnamed x27 -> x46, local copies, waits for them, and re-layouts: 5.8 us -> 24.1 us
    unnamed x4 -> x3, waiting for transfers between devices: 144 us -> 143 us
  transfers between devices with their start and end apart: 5 -> 7, of which waited for: 4 -> 6; matrix products, arithmetic and copies ran while one was open for 3% -> 3% of each run, Pallas kernels for 0% -> 0%
where the time goes in v1:
time: 417 us
  waiting for transfers between devices  258 us (62%)
  blocking collectives  55.5 us (13%)
  local copies, waits for them, and re-layouts  42.1 us (10%)
  matrix products  26.1 us (6%)
  between operations  14.5 us (3%)
  other arithmetic  11.5 us (3%)
  starting transfers between devices  9.16 us (2%)
    unnamed x3, waiting for transfers between devices  143 us
    ppermute x3, waiting for transfers between devices, per_device(): lax.ppermute(ring[-1], 'tp', [(dev, (dev + 1) % 4) for dev in range(4)])  76.8 us
    all_to_all x1, blocking collectives, per_device(): lax.all_to_all(buffer, 'ep', split_axis=0, concat_axis=0, tiled=True)  55.5 us
    unnamed x46, local copies, waits for them, and re-layouts  24.1 us
    all_gather x1, waiting for transfers between devices, per_device(): lax.all_gather(attended, 'tp', axis=1, tiled=True)  22.5 us
    all_to_all x1, waiting for transfers between devices, per_device(): lax.all_to_all(summed, 'ep', split_axis=0, concat_axis=0, tiled=True)  15.8 us
    dot_general x1, matrix products, per_device(): jnp.einsum('setcf,efd->setcd', activated, expert_down, preferred_element_...  13.5 us
  transfers between devices with their start and end apart: 7, of which 6 were waited for; matrix products, arithmetic and copies ran while one was open for 3% of the time, Pallas kernels for 0%

profile of v1, /device:TPU:0, one launch (start us, length us, event | category | flops | bytes accessed | tf_op | source)
XLA Modules:
  0.0 416.7 jit_solution(13291510029330505890)
XLA Ops:
  9.7 1.2 fusion.26
  10.9 1.3 fusion.28
  12.2 1.6 broadcast_in_dim.34
  13.8 2.3 reshape.383
  16.0 4.4 %scatter_custom_fusion = bf16[512,2048]{1,0:T(8,128)(2,1)} fusion(s32[256]{0:T(256)S(1)} %bitcast.169, bf16[256,2048]{1,0:T(8,128)(2,1)} %reshape.383, bf16[]{:T(256)} %constant.86.clone.1), kind=kCustom, calls=%fused_computation.36 | custom fusion | bytes 2097664 | tf_op jit(solution)/shard_map/scatter | solution.py:53
  20.5 55.5 %all_to_all.10 = bf16[8,2,1,32,2048]{4,3,2,1,0:T(8,128)(2,1)S(1)} all-to-all(bf16[8,2,1,32,2048]{4,3,2,1,0:T(8,128)(2,1)} %bitcast.157), channel_id=1, replica_groups=mesh['ep'=8,'tp'=4] {'ep'}, dimensions={0} | all-to-all | bytes 4194304 | tf_op jit(solution)/shard_map/all_to_all | solution.py:133
  76.0 1.3 copy-done.2
  77.6 25.4 %collective-permute-done.1 = bf16[8,2,1,32,2048]{4,3,2,0,1:T(8,128)(2,1)S(1)} collective-permute-done((bf16[8,2,1,32,2048]{4,3,2,0,1:T(8,128)(2,1)S(1)}, bf16[8,2,1,32,2048]{4,3,2,0,1:T(8,128)(2,1)S(1)}, u32[]{:S(2)}, u32[]{:S(2)}) %collective-permute-start.1) | collective-permute-done | bytes 2097184 | tf_op jit(solution)/shard_map/ppermute | solution.py:136
  103.0 1.3 copy-done.4
  104.4 25.6 %collective-permute-done.2 = bf16[8,2,1,32,2048]{4,3,2,0,1:T(8,128)(2,1)} collective-permute-done((bf16[8,2,1,32,2048]{4,3,2,0,1:T(8,128)(2,1)S(1)}, bf16[8,2,1,32,2048]{4,3,2,0,1:T(8,128)(2,1)}, u32[]{:S(2)}, u32[]{:S(2)}) %collective-permute-start.2) | collective-permute-done | bytes 2097184 | tf_op jit(solution)/shard_map/ppermute | solution.py:136
  130.0 25.8 %collective-permute-done.3 = bf16[8,2,1,32,2048]{4,3,2,0,1:T(8,128)(2,1)} collective-permute-done((bf16[8,2,1,32,2048]{4,3,2,0,1:T(8,128)(2,1)}, bf16[8,2,1,32,2048]{4,3,2,0,1:T(8,128)(2,1)}, u32[]{:S(2)}, u32[]{:S(2)}) %collective-permute-start.3) | collective-permute-done | bytes 2097184 | tf_op jit(solution)/shard_map/ppermute | solution.py:136
  155.7 1.8 constant_dynamic-update-slice_fusion.7
  157.6 2.0 constant_dynamic-update-slice_fusion.6
  159.9 1.4 copy-done.3
  161.5 1.8 constant_dynamic-update-slice_fusion.3
  163.4 1.8 constant_dynamic-update-slice_fusion.2
  165.5 6.1 %copy-done.10 = bf16[8,2,8,32,2048]{4,3,2,0,1:T(8,128)(2,1)} copy-done((bf16[8,2,8,32,2048]{4,3,2,0,1:T(8,128)(2,1)}, bf16[8,2,8,32,2048]{4,3,2,0,1:T(8,128)(2,1)S(1)}, u32[]{:S(2)}) %copy-start.10) | copy-done | bytes 16777240
  171.6 3.7 fusion.2
  175.3 13.5 %convert_bitcast_fusion = bf16[8,2,4,32,2048]{4,3,2,0,1:T(8,128)(2,1)} fusion(bf16[2,256,2048]{2,1,0:T(8,128)(2,1)S(1)} %copy-done, f32[2,8,4,32,256]{4,3,2,1,0:T(8,128)} %fusion.2, bf16[2,2048,256]{2,1,0:T(8,128)(2,1)} %param.24, bf16[8,2,8,32,2048]{4,3,2,0,1:T(8,128)(2,1)} %copy-done.10, s32[]{:T(128)S(6)} %select_n.54), kind=kOutput, calls=%fused_computation.2 | convolution fusion | flops 4302307328 | bytes 23068676 | tf_op jit(solution)/shard_map/setcf,efd->setcd/dot_general | solution.py:148
  189.8 3.5 collective-permute-start
  196.1 1.1 fusion.4
  198.1 142.8 %all-reduce.3.cloned.1.call-done = bf16[8,2,4,32,2048]{4,3,2,0,1:T(8,128)(2,1)} async-done(((bf16[8,2,4,32,2048]{4,3,2,0,1:T(8,128)(2,1)}), bf16[8,2,4,32,2048]{4,3,2,0,1:T(8,128)(2,1)}) %all-reduce.3.cloned.1.call-update) | async-done | bytes 8388624
  340.9 2.5 constant_dynamic-slice_fusion.1
  343.4 1.6 copy.74
  345.0 5.5 %all-to-all-start.1 = ((bf16[8,2,1,32,2048]{4,3,2,1,0:T(8,128)(2,1)}), bf16[8,2,1,32,2048]{4,3,2,1,0:T(8,128)(2,1)S(1)}, u32[]{:S(2)}, u32[]{:S(2)}) async-start(bf16[8,2,1,32,2048]{4,3,2,1,0:T(8,128)(2,1)} %copy.74), calls=%async_computation.1 | async-start | bytes 4194304 | tf_op jit(solution)/shard_map/all_to_all | solution.py:154
  350.5 3.4 fusion.23
  356.0 22.5 %all-gather.2.cloned.1.call-done = bf16[1024,1024]{0,1:T(8,128)(2,1)} async-done(((bf16[1024,256]{0,1:T(8,128)(2,1)}), bf16[1024,1024]{0,1:T(8,128)(2,1)}) %all-gather.2.cloned.1.call-update) | async-done | bytes 2097168 | tf_op jit(solution)/shard_map/all_gather | solution.py:116
  378.5 4.1 convolution_convert_fusion
  382.6 15.8 %all-to-all-done.1 = bf16[8,2,1,32,2048]{4,3,2,1,0:T(8,128)(2,1)S(1)} async-done(((bf16[8,2,1,32,2048]{4,3,2,1,0:T(8,128)(2,1)}), bf16[8,2,1,32,2048]{4,3,2,1,0:T(8,128)(2,1)S(1)}, u32[]{:S(2)}, u32[]{:S(2)}) %all-to-all-start.1) | async-done | bytes 2097184 | tf_op jit(solution)/shard_map/all_to_all | solution.py:154
  398.4 2.3 gather_fusion
  400.7 3.5 reshape.370
  404.3 5.6 %multiply_reduce_fusion = bf16[128,2048]{1,0:T(8,128)(2,1)} fusion(f32[128,2,2048]{2,1,0:T(2,128)} %reshape.370, f32[128,2]{1,0:T(8,128)S(1)} %copy.64), kind=kLoop, calls=%fused_computation.24 | loop fusion | flops 786432 | bytes 2622464 | tf_op jit(solution)/shard_map/reduce_sum | solution.py:159
  (95 shorter events, 10.1 us)
Async XLA Ops:
  7.2 168.2 %copy-start = (bf16[2,256,2048]{2,1,0:T(8,128)(2,1)S(1)}, bf16[2,256,2048]{2,1,0:T(8,128)(2,1)}, u32[]{:S(2)}) copy-start(bf16[2,256,2048]{2,1,0:T(8,128)(2,1)} %param.25) | copy-start | bytes 6291460
  7.2 333.7 %all-reduce.3.cloned.1.call-start = ((), (), s32[]{:S(2)}) async-start(), calls=%async_computation.3 | async-start | bytes 16777216
  76.0 1.3 copy-start.2
  77.5 25.5 %collective-permute-start.1 = (bf16[8,2,1,32,2048]{4,3,2,0,1:T(8,128)(2,1)S(1)}, bf16[8,2,1,32,2048]{4,3,2,0,1:T(8,128)(2,1)S(1)}, u32[]{:S(2)}, u32[]{:S(2)}) collective-permute-start(bf16[8,2,1,32,2048]{4,3,2,0,1:T(8,128)(2,1)S(1)} %copy.71), channel_id=1, source_target_pairs={{0,1},{1,2},{2,3},{3,0},{4,5},{5,6},{6,7},{7,4},{8,9},{9,10},{10,1... | collective-permute-start | bytes 6291464 | tf_op jit(solution)/shard_map/ppermute | solution.py:136
  103.0 1.3 copy-start.4
  104.4 25.6 %collective-permute-start.2 = (bf16[8,2,1,32,2048]{4,3,2,0,1:T(8,128)(2,1)S(1)}, bf16[8,2,1,32,2048]{4,3,2,0,1:T(8,128)(2,1)}, u32[]{:S(2)}, u32[]{:S(2)}) collective-permute-start(bf16[8,2,1,32,2048]{4,3,2,0,1:T(8,128)(2,1)S(1)} %collective-permute-done.1), channel_id=1, source_target_pairs={{0,1},{1,2},{2,3},{3,0},{4,5},{5,6},{6,7},{7,4},{8,9},{9,10},{10,1... | collective-permute-start | bytes 6291464 | tf_op jit(solution)/shard_map/ppermute | solution.py:136
  130.0 25.8 %collective-permute-start.3 = (bf16[8,2,1,32,2048]{4,3,2,0,1:T(8,128)(2,1)}, bf16[8,2,1,32,2048]{4,3,2,0,1:T(8,128)(2,1)}, u32[]{:S(2)}, u32[]{:S(2)}) collective-permute-start(bf16[8,2,1,32,2048]{4,3,2,0,1:T(8,128)(2,1)} %collective-permute-done.2), channel_id=1, source_target_pairs={{0,1},{1,2},{2,3},{3,0},{4,5},{5,6},{6,7},{7,4},{8,9},{9,10},{10,1... | collective-permute-start | bytes 6291464 | tf_op jit(solution)/shard_map/ppermute | solution.py:136
  157.6 2.2 copy-start.5
  159.8 1.6 copy-start.3
  165.3 6.3 %copy-start.14 = (bf16[2,2048,256]{2,1,0:T(8,128)(2,1)S(1)}, bf16[2,2048,256]{2,1,0:T(8,128)(2,1)}, u32[]{:S(2)}) copy-start(bf16[2,2048,256]{2,1,0:T(8,128)(2,1)} %param.23) | copy-start | bytes 6291460
  165.5 6.1 %copy-start.10 = (bf16[8,2,8,32,2048]{4,3,2,0,1:T(8,128)(2,1)}, bf16[8,2,8,32,2048]{4,3,2,0,1:T(8,128)(2,1)S(1)}, u32[]{:S(2)}) copy-start(bf16[8,2,8,32,2048]{4,3,2,0,1:T(8,128)(2,1)S(1)} %constant_dynamic-update-slice_fusion) | copy-start | bytes 50331652
  188.8 0.9 copy-start.7
  188.8 1.0 copy-start.8
  188.8 5.0 %copy-start.9 = (bf16[1024,256]{1,0:T(8,128)(2,1)S(1)}, bf16[1024,256]{1,0:T(8,128)(2,1)}, u32[]{:S(2)}) copy-start(bf16[1024,256]{1,0:T(8,128)(2,1)} %param.13) | copy-start | bytes 1572868
  189.8 4.6 %copy-start.15 = (u32[32]{0:T(128)S(1)}, u32[32]{0:T(128)}, u32[]{:S(2)}) copy-start(u32[32]{0:T(128)} %constant.96) | copy-start | bytes 388
  189.8 5.2 %collective-permute-start = (bf16[2,128,64]{1,2,0:T(8,128)(2,1)S(1)}, bf16[2,128,64]{1,2,0:T(8,128)(2,1)S(1)}, u32[]{:S(2)}, u32[]{:S(2)}) collective-permute-start(bf16[2,128,64]{1,2,0:T(8,128)(2,1)S(1)} %pad_maximum_fusion.2), channel_id=1, source_target_pairs={{0,4},{4,8},{8,12},{12,16},{16,20},{20,24},{24,28},{1,5},{5,9},{9,... | collective-permute-start | bytes 98312 | tf_op jit(solution)/shard_map/ppermute | solution.py:15
  195.1 0.9 copy-start.13
  196.0 2.0 copy-start.6
  345.0 53.4 %all-to-all-start.1 = ((bf16[8,2,1,32,2048]{4,3,2,1,0:T(8,128)(2,1)}), bf16[8,2,1,32,2048]{4,3,2,1,0:T(8,128)(2,1)S(1)}, u32[]{:S(2)}, u32[]{:S(2)}) async-start(bf16[8,2,1,32,2048]{4,3,2,1,0:T(8,128)(2,1)} %copy.74), calls=%async_computation.1 | async-start | bytes 4194304 | tf_op jit(solution)/shard_map/all_to_all | solution.py:154
  350.5 28.0 %all-gather.2.cloned.1.call-start = ((), (), s32[]{:S(2)}) async-start(), calls=%async_computation.2 | async-start | bytes 2621440 | tf_op jit(solution)/shard_map/all_gather | solution.py:116
  353.9 1.3 copy-start.11
  353.9 1.6 copy-start.12
  400.7 9.1 %copy-start.1 = (bf16[2,256,2048]{2,1,0:T(8,128)(2,1)S(1)}, bf16[2,256,2048]{2,1,0:T(8,128)(2,1)}, u32[]{:S(2)}) copy-start(bf16[2,256,2048]{2,1,0:T(8,128)(2,1)} %param.25) | copy-start | bytes 6291460
Sparse Core Ops, SparseCore 0:
  189.0 151.8 all-reduce.2
  355.3 23.1 all-gather.1
